TPU v7x, 32 devices: a whole 2x2x4 slice. The times are simulated.
32 devices in a mesh: ep: 8 (over z, x), tp: 4 (over y, core).
Axes of the slice: x: 2, y: 2, z: 4, core: 2. Of those that a mesh axis runs over, the one named last changes fastest.
Arguments:
- q_in: bfloat16 [4096, 1024], P('ep', 'tp'), may hold values from -6 to 6
- k_in: bfloat16 [4096, 256], P('ep'), may hold values from -6 to 6
- v_in: bfloat16 [4096, 256], P('ep'), may hold values from -6 to 6
- q_gain: float32 [64], replicated, may hold values from 0.1 to 1.9
- k_gain: float32 [64], replicated, may hold values from 0.1 to 1.9
- w_out: bfloat16 [1024, 2048], P('tp'), may hold values from -0.1875 to 0.1875
- post_gain: float32 [2048], replicated, may hold values from 0.1 to 1.9
- moe_in: bfloat16 [1024, 2048], P('ep'), may hold values from -6 to 6
- routes: int32 [1024, 2], P('ep'), may hold values from 0 to 7, all different within a row; in each aligned block of 128 rows (0 to 127, 128 to 255, ...) at most 48 rows name the same one
- route_logits: float32 [1024, 2], P('ep'), may hold values from -6 to 6
- pre_gain: float32 [2048], replicated, may hold values from 0.1 to 1.9
- w_gate: bfloat16 [8, 2048, 4096], P('ep', None, 'tp'), may hold values from -0.125 to 0.125
- w_up: bfloat16 [8, 2048, 4096], P('ep', None, 'tp'), may hold values from -0.125 to 0.125
- w_down: bfloat16 [8, 4096, 2048], P('ep', 'tp'), may hold values from -0.125 to 0.125
Outputs:
- attn_out: bfloat16 [4096, 2048], P(('ep', 'tp'))
- moe_out: bfloat16 [1024, 2048], P('ep', 'tp')
Inputs may be any that keep to these rules, and one draw needn't show every extreme that they name: `routes`: each row names 2 different experts. Among the rows of one index of ep no expert is named by more than 48 rows, a bound that some block reaches of them.
All inputs are finite; a program needn't handle non-finite values.
Results may differ from a plain program's by a relative error of at most 0.018.
Values may be sent and summed in bfloat16 or wider, within the bound.
A program may use at most 64 MiB of HBM per device.

v0:
```python
import jax
import jax.numpy as jnp
from jax import lax
from jax.sharding import PartitionSpec as P

GRID_W = 128
EPSILON = 1e-06
ROPE_BASE = 10000.0


def head_norm(values, gain):
    return values * lax.rsqrt(jnp.mean(values * values, axis=-1, keepdims=True) + EPSILON) * gain


def rotate_half(values, angles):
    quarter = angles.shape[-1]
    first_part = values[..., :quarter]
    second_part = values[..., quarter:]
    cosine = jnp.cos(angles)[:, None, :]
    sine_part = jnp.sin(angles)[:, None, :]
    return jnp.concatenate(
        [
            first_part * cosine - second_part * sine_part,
            second_part * cosine + first_part * sine_part,
        ],
        axis=-1,
    )


def grid_rotary(values, offset):
    row_count = values.shape[0]
    head_width = values.shape[-1]
    quarter = head_width // 4
    half_width = head_width // 2
    position = offset + jnp.arange(row_count, dtype=jnp.int32)
    grid_row = (position // GRID_W).astype(jnp.float32)
    grid_col = (position % GRID_W).astype(jnp.float32)
    inverse = ROPE_BASE ** (-jnp.arange(quarter, dtype=jnp.float32) / quarter)
    return jnp.concatenate(
        [
            rotate_half(values[..., :half_width], grid_row[:, None] * inverse[None, :]),
            rotate_half(values[..., half_width:], grid_col[:, None] * inverse[None, :]),
        ],
        axis=-1,
    )


def slot_table(route_rows, expert_count, capacity):
    token_count, top_count = route_rows.shape
    flat_routes = route_rows.reshape(-1)
    one_hot = (flat_routes[:, None] == jnp.arange(expert_count, dtype=jnp.int32)[None, :]).astype(
        jnp.int32
    )
    ranked = jnp.sum((jnp.cumsum(one_hot, axis=0) - 1) * one_hot, axis=1)
    placed = flat_routes * capacity + ranked
    slot_owner = jnp.full((expert_count * capacity,), token_count * top_count, dtype=jnp.int32)
    slot_owner = slot_owner.at[placed].set(jnp.arange(token_count * top_count, dtype=jnp.int32))
    return (slot_owner, placed)


def mixer_half(q_in, k_in, v_in, q_gain, k_gain, w_out, post_gain):
    head_size = q_gain.shape[0]
    row_count = q_in.shape[0]
    local_heads = q_in.shape[1] // head_size
    kv_count = k_in.shape[1] // head_size
    tp_count = lax.axis_size("tp")
    repeat = local_heads * tp_count // kv_count
    offset = lax.axis_index("ep") * row_count
    queries = head_norm(q_in.astype(jnp.float32).reshape(row_count, local_heads, head_size), q_gain)
    queries = grid_rotary(queries, offset).astype(jnp.bfloat16)
    query_rows = jnp.transpose(queries, (1, 0, 2)).reshape(local_heads * row_count, head_size)
    kv_index = lax.axis_index("tp") * local_heads // repeat
    own_keys = lax.dynamic_slice_in_dim(k_in, kv_index * head_size, head_size, 1)
    own_values = lax.dynamic_slice_in_dim(v_in, kv_index * head_size, head_size, 1)
    own_keys = head_norm(own_keys.astype(jnp.float32)[:, None, :], k_gain)
    own_keys = grid_rotary(own_keys, offset)[:, 0, :].astype(jnp.bfloat16)
    paired = jnp.concatenate([own_keys, own_values], axis=1)
    scale_factor = head_size ** (-0.5)

    def attend_block(running, key_block):
        block_keys = key_block[:, :head_size]
        block_values = key_block[:, head_size:]
        scores = (
            jnp.einsum("qd,kd->qk", query_rows, block_keys, preferred_element_type=jnp.float32)
            * scale_factor
        )
        weights = jnp.exp(scores)
        numer = running[0] + jnp.dot(
            weights.astype(jnp.bfloat16), block_values, preferred_element_type=jnp.float32
        )
        return (numer, running[1] + jnp.sum(weights, axis=1))

    zero_init = (
        jnp.zeros((local_heads * row_count, head_size), jnp.float32),
        jnp.zeros((local_heads * row_count,), jnp.float32),
    )
    running = zero_init
    gathered_piece = lax.all_gather(paired, "ep", axis=0, tiled=True)
    piece_rows = gathered_piece.shape[0]
    blocks = gathered_piece.reshape(piece_rows // 512, 512, gathered_piece.shape[1])

    def scan_block(partial_value, key_block):
        return (attend_block(partial_value, key_block), None)

    running, unused = lax.scan(scan_block, running, blocks)
    numer, denom = running
    head_out = (numer / denom[:, None]).astype(jnp.bfloat16)
    head_out = jnp.transpose(head_out.reshape(local_heads, row_count, head_size), (1, 0, 2))
    head_out = head_out.reshape(row_count, local_heads * head_size)
    mixed = lax.psum_scatter(
        jnp.dot(head_out, w_out, preferred_element_type=jnp.float32).astype(jnp.bfloat16),
        "tp",
        scatter_dimension=0,
        tiled=True,
    ).astype(jnp.float32)
    return head_norm(mixed, post_gain).astype(jnp.bfloat16)


def experts_half(moe_in, routes, route_logits, pre_gain, w_gate, w_up, w_down):
    token_count, top_count = routes.shape
    model_width = moe_in.shape[1]
    expert_count = lax.axis_size("ep")
    capacity = max(2, 3 * top_count * token_count // (2 * expert_count))
    tp_count = lax.axis_size("tp")
    slice_width = model_width // tp_count
    normed = head_norm(moe_in.astype(jnp.float32), pre_gain).astype(jnp.bfloat16)
    slot_owner, placed = slot_table(routes, expert_count, capacity)
    padded = jnp.concatenate([normed, jnp.zeros((1, model_width), jnp.bfloat16)], axis=0)
    outgoing = padded[slot_owner // top_count].reshape(expert_count, capacity, model_width)
    arrived = lax.all_to_all(outgoing, "ep", split_axis=0, concat_axis=0, tiled=True)
    arrived = arrived.reshape(expert_count * capacity, model_width)
    gate_pre = jnp.dot(arrived, w_gate[0], preferred_element_type=jnp.float32)
    up_pre = jnp.dot(arrived, w_up[0], preferred_element_type=jnp.float32)
    hidden = (jax.nn.silu(gate_pre) * up_pre).astype(jnp.bfloat16)
    partial_out = jnp.dot(hidden, w_down[0], preferred_element_type=jnp.float32)
    partial_out = partial_out.reshape(expert_count, capacity, model_width)
    summed = lax.psum_scatter(
        partial_out.astype(jnp.bfloat16), "tp", scatter_dimension=2, tiled=True
    )
    returned = lax.all_to_all(summed, "ep", split_axis=0, concat_axis=0, tiled=True)
    returned = returned.reshape(expert_count * capacity, slice_width)
    copies = returned[placed].reshape(token_count, top_count, slice_width).astype(jnp.float32)
    route_weight = jax.nn.softmax(route_logits, axis=-1)
    return jnp.sum(route_weight[..., None] * copies, axis=1).astype(jnp.bfloat16)


def per_device(
    q_in,
    k_in,
    v_in,
    q_gain,
    k_gain,
    w_out,
    post_gain,
    moe_in,
    routes,
    route_logits,
    pre_gain,
    w_gate,
    w_up,
    w_down,
):
    attn_out = mixer_half(q_in, k_in, v_in, q_gain, k_gain, w_out, post_gain)
    moe_out = experts_half(moe_in, routes, route_logits, pre_gain, w_gate, w_up, w_down)
    return (attn_out, moe_out)


def solution(mesh):
    return jax.shard_map(
        per_device,
        mesh=mesh,
        in_specs=(
            P("ep", "tp"),
            P("ep", None),
            P("ep", None),
            P(),
            P(),
            P("tp", None),
            P(),
            P("ep", None),
            P("ep", None),
            P("ep", None),
            P(),
            P("ep", None, "tp"),
            P("ep", None, "tp"),
            P("ep", "tp", None),
        ),
        out_specs=(P(("ep", "tp"), None), P("ep", "tp")),
        check_vma=False,
    )
```

profile of v0, /device:TPU:0, one launch (start us, length us, event | category | flops | bytes accessed | tf_op | source)
XLA Modules:
  0.0 186.0 jit_solution(11214696343545034479)
XLA Ops:
  8.0 0.9 copy.40
  9.2 0.7 broadcast_multiply_fusion
  9.9 0.6 reduce-window.6
  10.4 0.2 slice_reduce_fusion
  10.8 0.1 mul.344
  11.1 1.4 scatter_custom_fusion
  12.5 1.2 fusion.22
  13.7 1.2 fusion.24
  15.0 3.1 %gather_fusion = bf16[384,2048]{1,0:T(8,128)(2,1)} fusion(bf16[129,2048]{1,0:T(8,128)(2,1)S(1)} %concatenate.17, s32[1024]{0:T(1024)S(1)} %pad_clamp_fusion.1), kind=kCustom, calls=%fused_computation | custom fusion | bytes 3147264 | tf_op jit(solution)/shard_map/gather | solution.py:129
  18.2 7.4 %all-to-all-start = ((bf16[8,48,2048]{2,1,0:T(8,128)(2,1)}), bf16[8,48,2048]{2,1,0:T(8,128)(2,1)}, u32[]{:S(2)}, u32[]{:S(2)}) async-start(bf16[8,48,2048]{2,1,0:T(8,128)(2,1)} %bitcast.13), calls=%async_computation.1 | async-start | bytes 3145728 | tf_op jit(solution)/shard_map/all_to_all | solution.py:130
  25.7 0.1 constant_dynamic-slice_fusion
  26.2 0.3 fusion.43
  26.6 0.7 pad_maximum_fusion
  27.3 0.1 copy.33
  27.6 0.3 multiply_cosine_fusion.1
  28.1 0.3 copy.43
  28.4 50.5 %all-gather.2.cloned.1.call-done = bf16[4096,128]{0,1:T(8,128)(2,1)} async-done(((bf16[512,128]{0,1:T(8,128)(2,1)}), bf16[4096,128]{0,1:T(8,128)(2,1)}) %all-gather.2.cloned.1.call-update) | async-done | bytes 1048592 | tf_op jit(solution)/shard_map/all_gather | solution.py:98
  78.9 1.6 copy.42
  80.6 4.6 %fusion.12 = f32[384,1024]{1,0:T(8,128)S(1)} fusion(bf16[384,2048]{1,0:T(8,128)(2,1)} %bitcast.14, bf16[1,2048,1024]{2,1,0:T(8,128)(2,1)} %param.27), kind=kOutput, calls=%fused_computation.18 | convolution fusion | flops 1610612736 | bytes 7340032 | tf_op jit(solution)/shard_map/dot_general | solution.py:132
  85.2 3.5 %multiply_convert_fusion = bf16[384,1024]{1,0:T(8,128)(2,1)S(1)} fusion(f32[384,1024]{1,0:T(8,128)S(1)} %fusion.12, bf16[384,2048]{1,0:T(8,128)(2,1)} %bitcast.14, bf16[1,2048,1024]{2,1,0:T(8,128)(2,1)S(1)} %copy-done.8), kind=kOutput, calls=%fused_computation.22 | convolution fusion | flops 1612972032 | bytes 8126464 | tf_op jit(solution)/shard_map/dot_general | solution.py:133
  88.8 3.0 %fusion.14 = bf16[8,48,2048]{2,1,0:T(8,128)(2,1)} fusion(bf16[8,48,1024]{2,1,0:T(8,128)(2,1)S(1)} %bitcast.62, bf16[1,1024,2048]{2,1,0:T(8,128)(2,1)S(1)} %copy-done.9), kind=kOutput, calls=%fused_computation.21 | convolution fusion | flops 1611399168 | bytes 6553600 | tf_op jit(solution)/shard_map/dot_general | solution.py:135
  91.8 46.4 %while.13 = (s32[]{:T(128)}, f32[2048,64]{0,1:T(8,128)S(1)}, f32[2048]{0:T(1024)S(1)}, bf16[8,512,128]{2,1,0:T(8,128)(2,1)S(1)}, bf16[2048,64]{1,0:T(8,128)(2,1)S(1)}, /*index=5*/s32[]{:T(128)}, s32[]{:T(128)}) while((s32[]{:T(128)}, f32[2048,64]{0,1:T(8,128)S(1)}, f32[2048]{0:T(1024)S(1)}, bf16[8,512,128]{2,1,0:T(8,128)(2,1)S(1)}, ...), condition=%wide.region_4.5_spmd.clone, body=%wide.region_2.4_spmd.clone.sunk | while | flops 272893952 | bytes 10256476 | solution.py:105
  91.9 2.7 %fusion.72 = (f32[2048]{0:T(1024)S(1)}, f32[512,2048]{1,0:T(8,128)}) fusion(bf16[2048,64]{1,0:T(8,128)(2,1)S(1)} %get-tuple-element.147, bf16[512,128]{1,0:T(8,128)(2,1)S(1)} %dynamic-slice_bitcast_fusion.2), kind=kOutput, calls=%fused_computation.4.clone.1 | convolution fusion | flops 136312832 | bytes 4595712 | tf_op jit(solution)/shard_map/while/body/eval_jaxpr/qd,kd->qk/dot_general | solution.py:84
  94.5 3.1 %convolution_add_fusion.2 = f32[2048,64]{0,1:T(8,128)S(1)} fusion(f32[512,2048]{1,0:T(8,128)} %get-tuple-element.127, f32[2048,64]{0,1:T(8,128)S(1)} %get-tuple-element.137, pred[]{:T(512)S(6)} %compare.19, bf16[512,128]{1,0:T(8,128)(2,1)S(1)} %dynamic-slice_bitcast_fusion.2), kind=kOutput, calls=%fused_computation.6.clone.1 | convolution fusion | flops 136577024 | bytes 5373953 | tf_op jit(solution)/shard_map/while/body/eval_jaxpr/dot_general | solution.py:88
  97.7 2.7 %fusion.72 = (f32[2048]{0:T(1024)S(1)}, f32[512,2048]{1,0:T(8,128)}) fusion(bf16[2048,64]{1,0:T(8,128)(2,1)S(1)} %get-tuple-element.147, bf16[512,128]{1,0:T(8,128)(2,1)S(1)} %dynamic-slice_bitcast_fusion.2), kind=kOutput, calls=%fused_computation.4.clone.1 | convolution fusion | flops 136312832 | bytes 4595712 | tf_op jit(solution)/shard_map/while/body/eval_jaxpr/qd,kd->qk/dot_general | solution.py:84
  100.3 3.2 %convolution_add_fusion.2 = f32[2048,64]{0,1:T(8,128)S(1)} fusion(f32[512,2048]{1,0:T(8,128)} %get-tuple-element.127, f32[2048,64]{0,1:T(8,128)S(1)} %get-tuple-element.137, pred[]{:T(512)S(6)} %compare.19, bf16[512,128]{1,0:T(8,128)(2,1)S(1)} %dynamic-slice_bitcast_fusion.2), kind=kOutput, calls=%fused_computation.6.clone.1 | convolution fusion | flops 136577024 | bytes 5373953 | tf_op jit(solution)/shard_map/while/body/eval_jaxpr/dot_general | solution.py:88
  103.5 2.7 %fusion.72 = (f32[2048]{0:T(1024)S(1)}, f32[512,2048]{1,0:T(8,128)}) fusion(bf16[2048,64]{1,0:T(8,128)(2,1)S(1)} %get-tuple-element.147, bf16[512,128]{1,0:T(8,128)(2,1)S(1)} %dynamic-slice_bitcast_fusion.2), kind=kOutput, calls=%fused_computation.4.clone.1 | convolution fusion | flops 136312832 | bytes 4595712 | tf_op jit(solution)/shard_map/while/body/eval_jaxpr/qd,kd->qk/dot_general | solution.py:84
  106.2 3.1 %convolution_add_fusion.2 = f32[2048,64]{0,1:T(8,128)S(1)} fusion(f32[512,2048]{1,0:T(8,128)} %get-tuple-element.127, f32[2048,64]{0,1:T(8,128)S(1)} %get-tuple-element.137, pred[]{:T(512)S(6)} %compare.19, bf16[512,128]{1,0:T(8,128)(2,1)S(1)} %dynamic-slice_bitcast_fusion.2), kind=kOutput, calls=%fused_computation.6.clone.1 | convolution fusion | flops 136577024 | bytes 5373953 | tf_op jit(solution)/shard_map/while/body/eval_jaxpr/dot_general | solution.py:88
  109.3 2.7 %fusion.72 = (f32[2048]{0:T(1024)S(1)}, f32[512,2048]{1,0:T(8,128)}) fusion(bf16[2048,64]{1,0:T(8,128)(2,1)S(1)} %get-tuple-element.147, bf16[512,128]{1,0:T(8,128)(2,1)S(1)} %dynamic-slice_bitcast_fusion.2), kind=kOutput, calls=%fused_computation.4.clone.1 | convolution fusion | flops 136312832 | bytes 4595712 | tf_op jit(solution)/shard_map/while/body/eval_jaxpr/qd,kd->qk/dot_general | solution.py:84
  112.0 3.1 %convolution_add_fusion.2 = f32[2048,64]{0,1:T(8,128)S(1)} fusion(f32[512,2048]{1,0:T(8,128)} %get-tuple-element.127, f32[2048,64]{0,1:T(8,128)S(1)} %get-tuple-element.137, pred[]{:T(512)S(6)} %compare.19, bf16[512,128]{1,0:T(8,128)(2,1)S(1)} %dynamic-slice_bitcast_fusion.2), kind=kOutput, calls=%fused_computation.6.clone.1 | convolution fusion | flops 136577024 | bytes 5373953 | tf_op jit(solution)/shard_map/while/body/eval_jaxpr/dot_general | solution.py:88
  115.1 2.7 %fusion.72 = (f32[2048]{0:T(1024)S(1)}, f32[512,2048]{1,0:T(8,128)}) fusion(bf16[2048,64]{1,0:T(8,128)(2,1)S(1)} %get-tuple-element.147, bf16[512,128]{1,0:T(8,128)(2,1)S(1)} %dynamic-slice_bitcast_fusion.2), kind=kOutput, calls=%fused_computation.4.clone.1 | convolution fusion | flops 136312832 | bytes 4595712 | tf_op jit(solution)/shard_map/while/body/eval_jaxpr/qd,kd->qk/dot_general | solution.py:84
  117.8 3.1 %convolution_add_fusion.2 = f32[2048,64]{0,1:T(8,128)S(1)} fusion(f32[512,2048]{1,0:T(8,128)} %get-tuple-element.127, f32[2048,64]{0,1:T(8,128)S(1)} %get-tuple-element.137, pred[]{:T(512)S(6)} %compare.19, bf16[512,128]{1,0:T(8,128)(2,1)S(1)} %dynamic-slice_bitcast_fusion.2), kind=kOutput, calls=%fused_computation.6.clone.1 | convolution fusion | flops 136577024 | bytes 5373953 | tf_op jit(solution)/shard_map/while/body/eval_jaxpr/dot_general | solution.py:88
  120.9 2.7 %fusion.72 = (f32[2048]{0:T(1024)S(1)}, f32[512,2048]{1,0:T(8,128)}) fusion(bf16[2048,64]{1,0:T(8,128)(2,1)S(1)} %get-tuple-element.147, bf16[512,128]{1,0:T(8,128)(2,1)S(1)} %dynamic-slice_bitcast_fusion.2), kind=kOutput, calls=%fused_computation.4.clone.1 | convolution fusion | flops 136312832 | bytes 4595712 | tf_op jit(solution)/shard_map/while/body/eval_jaxpr/qd,kd->qk/dot_general | solution.py:84
  123.6 3.1 %convolution_add_fusion.2 = f32[2048,64]{0,1:T(8,128)S(1)} fusion(f32[512,2048]{1,0:T(8,128)} %get-tuple-element.127, f32[2048,64]{0,1:T(8,128)S(1)} %get-tuple-element.137, pred[]{:T(512)S(6)} %compare.19, bf16[512,128]{1,0:T(8,128)(2,1)S(1)} %dynamic-slice_bitcast_fusion.2), kind=kOutput, calls=%fused_computation.6.clone.1 | convolution fusion | flops 136577024 | bytes 5373953 | tf_op jit(solution)/shard_map/while/body/eval_jaxpr/dot_general | solution.py:88
  126.7 2.7 %fusion.72 = (f32[2048]{0:T(1024)S(1)}, f32[512,2048]{1,0:T(8,128)}) fusion(bf16[2048,64]{1,0:T(8,128)(2,1)S(1)} %get-tuple-element.147, bf16[512,128]{1,0:T(8,128)(2,1)S(1)} %dynamic-slice_bitcast_fusion.2), kind=kOutput, calls=%fused_computation.4.clone.1 | convolution fusion | flops 136312832 | bytes 4595712 | tf_op jit(solution)/shard_map/while/body/eval_jaxpr/qd,kd->qk/dot_general | solution.py:84
  129.4 3.1 %convolution_add_fusion.2 = f32[2048,64]{0,1:T(8,128)S(1)} fusion(f32[512,2048]{1,0:T(8,128)} %get-tuple-element.127, f32[2048,64]{0,1:T(8,128)S(1)} %get-tuple-element.137, pred[]{:T(512)S(6)} %compare.19, bf16[512,128]{1,0:T(8,128)(2,1)S(1)} %dynamic-slice_bitcast_fusion.2), kind=kOutput, calls=%fused_computation.6.clone.1 | convolution fusion | flops 136577024 | bytes 5373953 | tf_op jit(solution)/shard_map/while/body/eval_jaxpr/dot_general | solution.py:88
  132.5 2.7 %fusion.72 = (f32[2048]{0:T(1024)S(1)}, f32[512,2048]{1,0:T(8,128)}) fusion(bf16[2048,64]{1,0:T(8,128)(2,1)S(1)} %get-tuple-element.147, bf16[512,128]{1,0:T(8,128)(2,1)S(1)} %dynamic-slice_bitcast_fusion.2), kind=kOutput, calls=%fused_computation.4.clone.1 | convolution fusion | flops 136312832 | bytes 4595712 | tf_op jit(solution)/shard_map/while/body/eval_jaxpr/qd,kd->qk/dot_general | solution.py:84
  135.2 3.1 %convolution_add_fusion.2 = f32[2048,64]{0,1:T(8,128)S(1)} fusion(f32[512,2048]{1,0:T(8,128)} %get-tuple-element.127, f32[2048,64]{0,1:T(8,128)S(1)} %get-tuple-element.137, pred[]{:T(512)S(6)} %compare.19, bf16[512,128]{1,0:T(8,128)(2,1)S(1)} %dynamic-slice_bitcast_fusion.2), kind=kOutput, calls=%fused_computation.6.clone.1 | convolution fusion | flops 136577024 | bytes 5373953 | tf_op jit(solution)/shard_map/while/body/eval_jaxpr/dot_general | solution.py:88
  138.3 0.2 reshape.365
  138.6 2.1 %convolution_convert_fusion = bf16[512,2048]{1,0:T(8,128)(2,1)} fusion(bf16[512,256]{0,1:T(8,128)(2,1)S(1)} %bitcast.57, bf16[256,2048]{1,0:T(8,128)(2,1)S(1)} %copy-done), kind=kOutput, calls=%fused_computation.20 | convolution fusion | flops 537919488 | bytes 3407872 | tf_op jit(solution)/shard_map/dot_general | solution.py:111
  140.7 0.7 copy-done.4
  141.6 5.0 %all-to-all-start.1 = ((bf16[8,48,512]{2,1,0:T(8,128)(2,1)}), bf16[8,48,512]{2,1,0:T(8,128)(2,1)S(1)}, u32[]{:S(2)}, u32[]{:S(2)}) async-start(bf16[8,48,512]{2,1,0:T(8,128)(2,1)} %reduce-scatter.5.cloned.1.call-done), calls=%async_computation.3 | async-start | bytes 786432 | tf_op jit(solution)/shard_map/all_to_all | solution.py:140
  146.6 25.8 %reduce-scatter.3.cloned.1.call-done = bf16[128,2048]{1,0:T(8,128)(2,1)} async-done(((bf16[512,2048]{1,0:T(8,128)(2,1)}), bf16[128,2048]{1,0:T(8,128)(2,1)}) %reduce-scatter.3.cloned.1.call-update) | async-done | bytes 524304 | tf_op jit(solution)/shard_map/reduce_scatter | solution.py:110
  172.4 1.2 fusion.19
  173.7 2.0 %fusion.21 = bf16[128,2048]{1,0:T(8,128)(2,1)} fusion(bf16[128,2048]{1,0:T(8,128)(2,1)} %reduce-scatter.3.cloned.1.call-done, f32[2048]{0:T(1024)S(1)} %copy-done.5, f32[128]{0:T(128)S(1)} %add_rsqrt_fusion.3), kind=kLoop, calls=%fused_computation.29 | loop fusion | flops 1048576 | bytes 1057280 | tf_op jit(solution)/shard_map/convert_element_type | solution.py:116
  175.7 1.2 gather_fusion.1
  176.8 0.3 reshape.373
  177.2 1.4 multiply_reduce_fusion
  (80 shorter events, 1.9 us)
Async XLA Ops:
  8.0 130.6 %copy-start = (bf16[256,2048]{1,0:T(8,128)(2,1)S(1)}, bf16[256,2048]{1,0:T(8,128)(2,1)}, u32[]{:S(2)}) copy-start(bf16[256,2048]{1,0:T(8,128)(2,1)} %param.21) | copy-start | bytes 3145732
  18.1 7.5 %copy-start.2 = (bf16[512,256]{1,0:T(8,128)(2,1)S(1)}, bf16[512,256]{1,0:T(8,128)(2,1)}, u32[]{:S(2)}) copy-start(bf16[512,256]{1,0:T(8,128)(2,1)} %param.18) | copy-start | bytes 786436
  18.2 7.5 %copy-start.3 = (bf16[512,256]{1,0:T(8,128)(2,1)S(1)}, bf16[512,256]{1,0:T(8,128)(2,1)}, u32[]{:S(2)}) copy-start(bf16[512,256]{1,0:T(8,128)(2,1)} %param.17) | copy-start | bytes 786436
  18.2 8.0 %copy-start.6 = (f32[64]{0:T(128)S(1)}, f32[64]{0:T(128)}, u32[]{:S(2)}) copy-start(f32[64]{0:T(128)} %param.20) | copy-start | bytes 772
  18.2 9.2 %copy-start.1 = (bf16[512,256]{1,0:T(8,128)(2,1)S(1)}, bf16[512,256]{1,0:T(8,128)(2,1)}, u32[]{:S(2)}) copy-start(bf16[512,256]{1,0:T(8,128)(2,1)} %param.16) | copy-start | bytes 786436
  18.2 62.4 %all-to-all-start = ((bf16[8,48,2048]{2,1,0:T(8,128)(2,1)}), bf16[8,48,2048]{2,1,0:T(8,128)(2,1)}, u32[]{:S(2)}, u32[]{:S(2)}) async-start(bf16[8,48,2048]{2,1,0:T(8,128)(2,1)} %bitcast.13), calls=%async_computation.1 | async-start | bytes 3145728 | tf_op jit(solution)/shard_map/all_to_all | solution.py:130
  25.6 2.3 %copy-start.7 = (f32[64]{0:T(128)S(1)}, f32[64]{0:T(128)}, u32[]{:S(2)}) copy-start(f32[64]{0:T(128)} %param.19) | copy-start | bytes 772
  25.6 53.3 %all-gather.2.cloned.1.call-start = ((), (), s32[]{:S(2)}) async-start(), calls=%async_computation.4 | async-start | bytes 1179648 | tf_op jit(solution)/shard_map/all_gather | solution.py:98
  27.2 114.3 %reduce-scatter.5.cloned.1.call-start = ((), (), s32[]{:S(2)}) async-start(), calls=%async_computation.6 | async-start | bytes 1966080 | tf_op jit(solution)/shard_map/reduce_scatter | solution.py:137
  80.6 4.6 %copy-start.8 = (bf16[1,2048,1024]{2,1,0:T(8,128)(2,1)S(1)}, bf16[1,2048,1024]{2,1,0:T(8,128)(2,1)}, u32[]{:S(2)}) copy-start(bf16[1,2048,1024]{2,1,0:T(8,128)(2,1)} %param.28) | copy-start | bytes 12582916
  85.2 3.6 %copy-start.9 = (bf16[1,1024,2048]{2,1,0:T(8,128)(2,1)S(1)}, bf16[1,1024,2048]{2,1,0:T(8,128)(2,1)}, u32[]{:S(2)}) copy-start(bf16[1,1024,2048]{2,1,0:T(8,128)(2,1)} %param.29) | copy-start | bytes 12582916
  91.8 80.6 %reduce-scatter.3.cloned.1.call-start = ((), (), s32[]{:S(2)}) async-start(), calls=%async_computation.5 | async-start | bytes 2621440 | tf_op jit(solution)/shard_map/reduce_scatter | solution.py:110
  140.7 0.7 copy-start.4
  140.7 33.0 %copy-start.5 = (f32[2048]{0:T(1024)S(1)}, f32[2048]{0:T(1024)}, u32[]{:S(2)}) copy-start(f32[2048]{0:T(1024)} %param.22) | copy-start | bytes 24580
  141.6 34.1 %all-to-all-start.1 = ((bf16[8,48,512]{2,1,0:T(8,128)(2,1)}), bf16[8,48,512]{2,1,0:T(8,128)(2,1)S(1)}, u32[]{:S(2)}, u32[]{:S(2)}) async-start(bf16[8,48,512]{2,1,0:T(8,128)(2,1)} %reduce-scatter.5.cloned.1.call-done), calls=%async_computation.3 | async-start | bytes 786432 | tf_op jit(solution)/shard_map/all_to_all | solution.py:140
Sparse Core Ops, SparseCore 0:
  29.0 49.8 all-gather.1
Sparse Core Ops, SparseCore 1:
  91.9 28.3 reduce-scatter.4
  140.8 31.6 reduce-scatter.2
where the time goes:
time: 187 us; the launch traced here: 186 us
  waiting for transfers between devices  76.5 us (41%)
  matrix products  59.2 us (32%)
  between operations  15.9 us (9%)
  starting transfers between devices  12.5 us (7%)
  local copies, waits for them, and re-layouts  11.2 us (6%)
  other arithmetic  10.4 us (6%)
    all_gather x1, waiting for transfers between devices, mixer_half(): gathered_piece = lax.all_gather(paired, 'ep', axis=0, tiled=True)  50.5 us
    reduce_scatter x1, waiting for transfers between devices, mixer_half(): lax.psum_scatter(jnp.dot(head_out, w_out, preferred_element_type=jnp.floa...  25.8 us
    dot_general x8, matrix products, attend_block(): jnp.dot(weights.astype(jnp.bfloat16), block_values, preferred_element_typ...  24.7 us
    dot_general x8, matrix products, attend_block(): jnp.einsum('qd,kd->qk', query_rows, block_keys, preferred_element_type=jn...  21.2 us
    all_to_all x1, starting transfers between devices, experts_half(): lax.all_to_all(outgoing, 'ep', split_axis=0, concat_axis=0, tiled=True)  7.42 us
    all_to_all x1, starting transfers between devices, experts_half(): lax.all_to_all(summed, 'ep', split_axis=0, concat_axis=0, tiled=True)  4.98 us
    dot_general x1, matrix products, experts_half(): gate_pre = jnp.dot(arrived, w_gate[0], preferred_element_type=jnp.float32)  4.59 us
    unnamed x26, local copies, waits for them, and re-layouts  3.79 us
  transfers between devices with their start and end apart: 5, of which 2 were waited for; matrix products, arithmetic and copies ran while one was open for 30% of the time, Pallas kernels for 0%

commit v1 on v0

--- a/solution.py
+++ b/solution.py
@@ -95,7 +95,14 @@
         jnp.zeros((local_heads * row_count,), jnp.float32),
     )
     running = zero_init
-    gathered_piece = lax.all_gather(paired, "ep", axis=0, tiled=True)
+    ways, here = (lax.axis_size("ep"), lax.axis_index("ep"))
+    gathered_piece, reach = (paired, 1)
+    while reach < ways:
+        theirs = lax.ppermute(gathered_piece, "ep", [(d, d ^ reach) for d in range(ways)])
+        mine_first = jnp.concatenate([gathered_piece, theirs], axis=0)
+        theirs_first = jnp.concatenate([theirs, gathered_piece], axis=0)
+        gathered_piece = jnp.where(here & reach == 0, mine_first, theirs_first)
+        reach = 2 * reach
     piece_rows = gathered_piece.shape[0]
     blocks = gathered_piece.reshape(piece_rows // 512, 512, gathered_piece.shape[1])
 

time: 187 us -> 233 us (1.25)
  waiting for transfers between devices: 76.5 us -> 109 us
  starting transfers between devices: 12.5 us -> 20.1 us
  local copies, waits for them, and re-layouts: 11.2 us -> 18.5 us
    ppermute x0 -> x3, waiting for transfers between devices: none -> 51.6 us  [mixer_half(): lax.ppermute(gathered_piece, 'ep', [(d, d ^ reach) for d in range(ways)])]
    all_gather x1 -> x0, waiting for transfers between devices: 50.5 us -> none  [mixer_half(): gathered_piece = lax.all_gather(paired, 'ep', axis=0, tiled=True)]
    reduce_scatter x1, waiting for transfers between devices: 0.03 us -> 29.3 us  [experts_half(): lax.psum_scatter(partial_out.astype(jnp.bfloat16), 'tp', scatter_dimensio...]
    all_to_all x1, waiting for transfers between devices: 0.01 us -> 9.53 us  [experts_half(): lax.all_to_all(summed, 'ep', split_axis=0, concat_axis=0, tiled=True)]
    ppermute x0 -> x3, starting transfers between devices: none -> 9.35 us  [mixer_half(): lax.ppermute(gathered_piece, 'ep', [(d, d ^ reach) for d in range(ways)])]
    reduce_scatter x1, waiting for transfers between devices: 25.8 us -> 18.6 us  [mixer_half(): lax.psum_scatter(jnp.dot(head_out, w_out, preferred_element_type=jnp.floa...]
    squeeze x8, local copies, waits for them, and re-layouts: 0.12 us -> 7.33 us  [mixer_half(): running, unused = lax.scan(scan_block, running, blocks)]
    all_to_all x1, starting transfers between devices: 7.42 us -> 5.01 us  [experts_half(): lax.all_to_all(outgoing, 'ep', split_axis=0, concat_axis=0, tiled=True)]
  transfers between devices with their start and end apart: 5 -> 7, of which waited for: 2 -> 5; matrix products, arithmetic and copies ran while one was open for 30% -> 36% of each run, Pallas kernels for 0% -> 0%
where the time goes in v1:
time: 233 us; the launch traced here: 232 us
  waiting for transfers between devices  109 us (47%)
  matrix products  59.1 us (25%)
  starting transfers between devices  20.1 us (9%)
  local copies, waits for them, and re-layouts  18.5 us (8%)
  between operations  14.5 us (6%)
  other arithmetic  10.3 us (4%)
    ppermute x3, waiting for transfers between devices, mixer_half(): lax.ppermute(gathered_piece, 'ep', [(d, d ^ reach) for d in range(ways)])  51.6 us
    reduce_scatter x1, waiting for transfers between devices, experts_half(): lax.psum_scatter(partial_out.astype(jnp.bfloat16), 'tp', scatter_dimensio...  29.3 us
    dot_general x8, matrix products, attend_block(): jnp.dot(weights.astype(jnp.bfloat16), block_values, preferred_element_typ...  24.6 us
    dot_general x8, matrix products, attend_block(): jnp.einsum('qd,kd->qk', query_rows, block_keys, preferred_element_type=jn...  21.2 us
    reduce_scatter x1, waiting for transfers between devices, mixer_half(): lax.psum_scatter(jnp.dot(head_out, w_out, preferred_element_type=jnp.floa...  18.6 us
    all_to_all x1, waiting for transfers between devices, experts_half(): lax.all_to_all(summed, 'ep', split_axis=0, concat_axis=0, tiled=True)  9.53 us
    ppermute x3, starting transfers between devices, mixer_half(): lax.ppermute(gathered_piece, 'ep', [(d, d ^ reach) for d in range(ways)])  9.35 us
    squeeze x8, local copies, waits for them, and re-layouts, mixer_half(): running, unused = lax.scan(scan_block, running, blocks)  7.33 us
  transfers between devices with their start and end apart: 7, of which 5 were waited for; matrix products, arithmetic and copies ran while one was open for 36% of the time, Pallas kernels for 0%

profile of v1, /device:TPU:0, one launch (start us, length us, event | category | flops | bytes accessed | tf_op | source)
XLA Modules:
  0.0 231.9 jit_solution(6665707826251025108)
XLA Ops:
  7.3 1.2 constant_dynamic-slice_fusion
  9.8 3.0 %collective-permute-start = (bf16[512,128]{0,1:T(8,128)(2,1)S(1)}, bf16[512,128]{0,1:T(8,128)(2,1)S(1)}, u32[]{:S(2)}, u32[]{:S(2)}) collective-permute-start(bf16[512,128]{0,1:T(8,128)(2,1)S(1)} %pad_maximum_fusion), channel_id=1, source_target_pairs={{0,4},{4,0},{8,12},{12,8},{16,20},{20,16},{24,28},{28,24},{1,5},{5... | collective-permute-start | bytes 393224 | tf_op jit(solution)/shard_map/ppermute | solution.py:101
  15.8 1.4 scatter_custom_fusion
  17.7 3.1 %gather_fusion = bf16[384,2048]{1,0:T(8,128)(2,1)} fusion(bf16[129,2048]{1,0:T(8,128)(2,1)S(1)} %concatenate.41, s32[1024]{0:T(1024)S(1)} %pad_clamp_fusion.1), kind=kCustom, calls=%fused_computation | custom fusion | bytes 3147264 | tf_op jit(solution)/shard_map/gather | solution.py:136
  20.9 5.0 %all-to-all-start = ((bf16[8,48,2048]{2,1,0:T(8,128)(2,1)}), bf16[8,48,2048]{2,1,0:T(8,128)(2,1)}, u32[]{:S(2)}, u32[]{:S(2)}) async-start(bf16[8,48,2048]{2,1,0:T(8,128)(2,1)} %bitcast.13), calls=%async_computation.1 | async-start | bytes 3145728 | tf_op jit(solution)/shard_map/all_to_all | solution.py:137
  26.3 2.0 collective-permute-start.1
  28.5 28.7 %collective-permute-done.1 = bf16[1024,128]{0,1:T(8,128)(2,1)S(1)} collective-permute-done((bf16[1024,128]{0,1:T(8,128)(2,1)S(1)}, bf16[1024,128]{0,1:T(8,128)(2,1)S(1)}, u32[]{:S(2)}, u32[]{:S(2)}) %collective-permute-start.1) | collective-permute-done | bytes 262176 | tf_op jit(solution)/shard_map/ppermute | solution.py:101
  57.3 4.3 %collective-permute-start.2 = (bf16[2048,128]{0,1:T(8,128)(2,1)S(1)}, bf16[2048,128]{0,1:T(8,128)(2,1)}, u32[]{:S(2)}, u32[]{:S(2)}) collective-permute-start(bf16[2048,128]{0,1:T(8,128)(2,1)S(1)} %maximum_select_fusion.1), channel_id=1, source_target_pairs={{0,16},{4,20},{8,24},{12,28},{16,0},{20,4},{24,8},{28,12},{1,17},{... | collective-permute-start | bytes 1572872 | tf_op jit(solution)/shard_map/ppermute | solution.py:101
  62.3 22.9 %collective-permute-done.2 = bf16[2048,128]{0,1:T(8,128)(2,1)} collective-permute-done((bf16[2048,128]{0,1:T(8,128)(2,1)S(1)}, bf16[2048,128]{0,1:T(8,128)(2,1)}, u32[]{:S(2)}, u32[]{:S(2)}) %collective-permute-start.2) | collective-permute-done | bytes 524320 | tf_op jit(solution)/shard_map/ppermute | solution.py:101
  85.2 1.8 maximum_select_fusion
  87.0 1.3 copy.42
  88.3 53.4 %while.13 = (s32[]{:T(128)}, f32[2048,64]{0,1:T(8,128)S(1)}, f32[2048]{0:T(1024)S(1)}, bf16[8,512,128]{2,1,0:T(8,128)(2,1)}, bf16[2048,64]{1,0:T(8,128)(2,1)S(1)}, /*index=5*/s32[]{:T(128)}, s32[]{:T(128)}) while((s32[]{:T(128)}, f32[2048,64]{0,1:T(8,128)S(1)}, f32[2048]{0:T(1024)S(1)}, bf16[8,512,128]{2,1,0:T(8,128)(2,1)}, ...), condition=%wide.region_4.5_spmd.clone, body=%wide.region_2.4_spmd.clone.sunk | while | flops 272893952 | bytes 10256476 | solution.py:112
  88.3 0.9 dynamic-slice_bitcast_fusion.2
  89.2 2.7 %fusion.72 = (f32[2048]{0:T(1024)S(1)}, f32[512,2048]{1,0:T(8,128)}) fusion(bf16[2048,64]{1,0:T(8,128)(2,1)S(1)} %get-tuple-element.147, bf16[512,128]{1,0:T(8,128)(2,1)S(1)} %dynamic-slice_bitcast_fusion.2), kind=kOutput, calls=%fused_computation.4.clone.1 | convolution fusion | flops 136312832 | bytes 4595712 | tf_op jit(solution)/shard_map/while/body/eval_jaxpr/qd,kd->qk/dot_general | solution.py:84
  91.9 3.1 %convolution_add_fusion.2 = f32[2048,64]{0,1:T(8,128)S(1)} fusion(f32[512,2048]{1,0:T(8,128)} %get-tuple-element.127, f32[2048,64]{0,1:T(8,128)S(1)} %get-tuple-element.137, pred[]{:T(512)S(6)} %compare.19, bf16[512,128]{1,0:T(8,128)(2,1)S(1)} %dynamic-slice_bitcast_fusion.2), kind=kOutput, calls=%fused_computation.6.clone.1 | convolution fusion | flops 136577024 | bytes 5373953 | tf_op jit(solution)/shard_map/while/body/eval_jaxpr/dot_general | solution.py:88
  95.0 0.9 dynamic-slice_bitcast_fusion.2
  95.9 2.7 %fusion.72 = (f32[2048]{0:T(1024)S(1)}, f32[512,2048]{1,0:T(8,128)}) fusion(bf16[2048,64]{1,0:T(8,128)(2,1)S(1)} %get-tuple-element.147, bf16[512,128]{1,0:T(8,128)(2,1)S(1)} %dynamic-slice_bitcast_fusion.2), kind=kOutput, calls=%fused_computation.4.clone.1 | convolution fusion | flops 136312832 | bytes 4595712 | tf_op jit(solution)/shard_map/while/body/eval_jaxpr/qd,kd->qk/dot_general | solution.py:84
  98.6 3.1 %convolution_add_fusion.2 = f32[2048,64]{0,1:T(8,128)S(1)} fusion(f32[512,2048]{1,0:T(8,128)} %get-tuple-element.127, f32[2048,64]{0,1:T(8,128)S(1)} %get-tuple-element.137, pred[]{:T(512)S(6)} %compare.19, bf16[512,128]{1,0:T(8,128)(2,1)S(1)} %dynamic-slice_bitcast_fusion.2), kind=kOutput, calls=%fused_computation.6.clone.1 | convolution fusion | flops 136577024 | bytes 5373953 | tf_op jit(solution)/shard_map/while/body/eval_jaxpr/dot_general | solution.py:88
  101.7 0.9 dynamic-slice_bitcast_fusion.2
  102.6 2.7 %fusion.72 = (f32[2048]{0:T(1024)S(1)}, f32[512,2048]{1,0:T(8,128)}) fusion(bf16[2048,64]{1,0:T(8,128)(2,1)S(1)} %get-tuple-element.147, bf16[512,128]{1,0:T(8,128)(2,1)S(1)} %dynamic-slice_bitcast_fusion.2), kind=kOutput, calls=%fused_computation.4.clone.1 | convolution fusion | flops 136312832 | bytes 4595712 | tf_op jit(solution)/shard_map/while/body/eval_jaxpr/qd,kd->qk/dot_general | solution.py:84
  105.2 3.1 %convolution_add_fusion.2 = f32[2048,64]{0,1:T(8,128)S(1)} fusion(f32[512,2048]{1,0:T(8,128)} %get-tuple-element.127, f32[2048,64]{0,1:T(8,128)S(1)} %get-tuple-element.137, pred[]{:T(512)S(6)} %compare.19, bf16[512,128]{1,0:T(8,128)(2,1)S(1)} %dynamic-slice_bitcast_fusion.2), kind=kOutput, calls=%fused_computation.6.clone.1 | convolution fusion | flops 136577024 | bytes 5373953 | tf_op jit(solution)/shard_map/while/body/eval_jaxpr/dot_general | solution.py:88
  108.3 0.9 dynamic-slice_bitcast_fusion.2
  109.3 2.7 %fusion.72 = (f32[2048]{0:T(1024)S(1)}, f32[512,2048]{1,0:T(8,128)}) fusion(bf16[2048,64]{1,0:T(8,128)(2,1)S(1)} %get-tuple-element.147, bf16[512,128]{1,0:T(8,128)(2,1)S(1)} %dynamic-slice_bitcast_fusion.2), kind=kOutput, calls=%fused_computation.4.clone.1 | convolution fusion | flops 136312832 | bytes 4595712 | tf_op jit(solution)/shard_map/while/body/eval_jaxpr/qd,kd->qk/dot_general | solution.py:84
  111.9 3.1 %convolution_add_fusion.2 = f32[2048,64]{0,1:T(8,128)S(1)} fusion(f32[512,2048]{1,0:T(8,128)} %get-tuple-element.127, f32[2048,64]{0,1:T(8,128)S(1)} %get-tuple-element.137, pred[]{:T(512)S(6)} %compare.19, bf16[512,128]{1,0:T(8,128)(2,1)S(1)} %dynamic-slice_bitcast_fusion.2), kind=kOutput, calls=%fused_computation.6.clone.1 | convolution fusion | flops 136577024 | bytes 5373953 | tf_op jit(solution)/shard_map/while/body/eval_jaxpr/dot_general | solution.py:88
  115.0 0.9 dynamic-slice_bitcast_fusion.2
  115.9 2.7 %fusion.72 = (f32[2048]{0:T(1024)S(1)}, f32[512,2048]{1,0:T(8,128)}) fusion(bf16[2048,64]{1,0:T(8,128)(2,1)S(1)} %get-tuple-element.147, bf16[512,128]{1,0:T(8,128)(2,1)S(1)} %dynamic-slice_bitcast_fusion.2), kind=kOutput, calls=%fused_computation.4.clone.1 | convolution fusion | flops 136312832 | bytes 4595712 | tf_op jit(solution)/shard_map/while/body/eval_jaxpr/qd,kd->qk/dot_general | solution.py:84
  118.6 3.1 %convolution_add_fusion.2 = f32[2048,64]{0,1:T(8,128)S(1)} fusion(f32[512,2048]{1,0:T(8,128)} %get-tuple-element.127, f32[2048,64]{0,1:T(8,128)S(1)} %get-tuple-element.137, pred[]{:T(512)S(6)} %compare.19, bf16[512,128]{1,0:T(8,128)(2,1)S(1)} %dynamic-slice_bitcast_fusion.2), kind=kOutput, calls=%fused_computation.6.clone.1 | convolution fusion | flops 136577024 | bytes 5373953 | tf_op jit(solution)/shard_map/while/body/eval_jaxpr/dot_general | solution.py:88
  121.7 0.9 dynamic-slice_bitcast_fusion.2
  122.6 2.7 %fusion.72 = (f32[2048]{0:T(1024)S(1)}, f32[512,2048]{1,0:T(8,128)}) fusion(bf16[2048,64]{1,0:T(8,128)(2,1)S(1)} %get-tuple-element.147, bf16[512,128]{1,0:T(8,128)(2,1)S(1)} %dynamic-slice_bitcast_fusion.2), kind=kOutput, calls=%fused_computation.4.clone.1 | convolution fusion | flops 136312832 | bytes 4595712 | tf_op jit(solution)/shard_map/while/body/eval_jaxpr/qd,kd->qk/dot_general | solution.py:84
  125.3 3.1 %convolution_add_fusion.2 = f32[2048,64]{0,1:T(8,128)S(1)} fusion(f32[512,2048]{1,0:T(8,128)} %get-tuple-element.127, f32[2048,64]{0,1:T(8,128)S(1)} %get-tuple-element.137, pred[]{:T(512)S(6)} %compare.19, bf16[512,128]{1,0:T(8,128)(2,1)S(1)} %dynamic-slice_bitcast_fusion.2), kind=kOutput, calls=%fused_computation.6.clone.1 | convolution fusion | flops 136577024 | bytes 5373953 | tf_op jit(solution)/shard_map/while/body/eval_jaxpr/dot_general | solution.py:88
  128.4 0.9 dynamic-slice_bitcast_fusion.2
  129.3 2.7 %fusion.72 = (f32[2048]{0:T(1024)S(1)}, f32[512,2048]{1,0:T(8,128)}) fusion(bf16[2048,64]{1,0:T(8,128)(2,1)S(1)} %get-tuple-element.147, bf16[512,128]{1,0:T(8,128)(2,1)S(1)} %dynamic-slice_bitcast_fusion.2), kind=kOutput, calls=%fused_computation.4.clone.1 | convolution fusion | flops 136312832 | bytes 4595712 | tf_op jit(solution)/shard_map/while/body/eval_jaxpr/qd,kd->qk/dot_general | solution.py:84
  132.0 3.1 %convolution_add_fusion.2 = f32[2048,64]{0,1:T(8,128)S(1)} fusion(f32[512,2048]{1,0:T(8,128)} %get-tuple-element.127, f32[2048,64]{0,1:T(8,128)S(1)} %get-tuple-element.137, pred[]{:T(512)S(6)} %compare.19, bf16[512,128]{1,0:T(8,128)(2,1)S(1)} %dynamic-slice_bitcast_fusion.2), kind=kOutput, calls=%fused_computation.6.clone.1 | convolution fusion | flops 136577024 | bytes 5373953 | tf_op jit(solution)/shard_map/while/body/eval_jaxpr/dot_general | solution.py:88
  135.1 0.9 dynamic-slice_bitcast_fusion.2
  136.0 2.7 %fusion.72 = (f32[2048]{0:T(1024)S(1)}, f32[512,2048]{1,0:T(8,128)}) fusion(bf16[2048,64]{1,0:T(8,128)(2,1)S(1)} %get-tuple-element.147, bf16[512,128]{1,0:T(8,128)(2,1)S(1)} %dynamic-slice_bitcast_fusion.2), kind=kOutput, calls=%fused_computation.4.clone.1 | convolution fusion | flops 136312832 | bytes 4595712 | tf_op jit(solution)/shard_map/while/body/eval_jaxpr/qd,kd->qk/dot_general | solution.py:84
  138.6 3.1 %convolution_add_fusion.2 = f32[2048,64]{0,1:T(8,128)S(1)} fusion(f32[512,2048]{1,0:T(8,128)} %get-tuple-element.127, f32[2048,64]{0,1:T(8,128)S(1)} %get-tuple-element.137, pred[]{:T(512)S(6)} %compare.19, bf16[512,128]{1,0:T(8,128)(2,1)S(1)} %dynamic-slice_bitcast_fusion.2), kind=kOutput, calls=%fused_computation.6.clone.1 | convolution fusion | flops 136577024 | bytes 5373953 | tf_op jit(solution)/shard_map/while/body/eval_jaxpr/dot_general | solution.py:88
  142.1 2.1 convolution_convert_fusion
  144.4 4.6 %fusion.12 = f32[384,1024]{1,0:T(8,128)S(1)} fusion(bf16[384,2048]{1,0:T(8,128)(2,1)} %bitcast.14, bf16[1,2048,1024]{2,1,0:T(8,128)(2,1)} %param.27), kind=kOutput, calls=%fused_computation.18 | convolution fusion | flops 1610612736 | bytes 7340032 | tf_op jit(solution)/shard_map/dot_general | solution.py:139
  149.1 3.6 %multiply_convert_fusion = bf16[384,1024]{1,0:T(8,128)(2,1)S(1)} fusion(f32[384,1024]{1,0:T(8,128)S(1)} %fusion.12, bf16[384,2048]{1,0:T(8,128)(2,1)} %bitcast.14, bf16[1,2048,1024]{2,1,0:T(8,128)(2,1)S(1)} %copy-done.8), kind=kOutput, calls=%fused_computation.22 | convolution fusion | flops 1612972032 | bytes 8126464 | tf_op jit(solution)/shard_map/dot_general | solution.py:140
  152.7 3.0 %fusion.14 = bf16[8,48,2048]{2,1,0:T(8,128)(2,1)} fusion(bf16[8,48,1024]{2,1,0:T(8,128)(2,1)S(1)} %bitcast.62, bf16[1,1024,2048]{2,1,0:T(8,128)(2,1)S(1)} %copy-done.9), kind=kOutput, calls=%fused_computation.21 | convolution fusion | flops 1611399168 | bytes 6553600 | tf_op jit(solution)/shard_map/dot_general | solution.py:142
  155.9 18.6 %reduce-scatter.3.cloned.1.call-done = bf16[128,2048]{1,0:T(8,128)(2,1)} async-done(((bf16[512,2048]{1,0:T(8,128)(2,1)}), bf16[128,2048]{1,0:T(8,128)(2,1)}) %reduce-scatter.3.cloned.1.call-update) | async-done | bytes 524304 | tf_op jit(solution)/shard_map/reduce_scatter | solution.py:117
  174.6 1.2 fusion.19
  175.8 29.3 %reduce-scatter.5.cloned.1.call-done = bf16[8,48,512]{2,1,0:T(8,128)(2,1)} async-done(((bf16[8,48,2048]{2,1,0:T(8,128)(2,1)}), bf16[8,48,512]{2,1,0:T(8,128)(2,1)}) %reduce-scatter.5.cloned.1.call-update) | async-done | bytes 393232 | tf_op jit(solution)/shard_map/reduce_scatter | solution.py:144
  205.1 5.5 %all-to-all-start.1 = ((bf16[8,48,512]{2,1,0:T(8,128)(2,1)}), bf16[8,48,512]{2,1,0:T(8,128)(2,1)S(1)}, u32[]{:S(2)}, u32[]{:S(2)}) async-start(bf16[8,48,512]{2,1,0:T(8,128)(2,1)} %reduce-scatter.5.cloned.1.call-done), calls=%async_computation.3 | async-start | bytes 786432 | tf_op jit(solution)/shard_map/all_to_all | solution.py:147
  210.6 2.0 fusion.21
  212.7 9.5 %all-to-all-done.1 = bf16[8,48,512]{2,1,0:T(8,128)(2,1)S(1)} async-done(((bf16[8,48,512]{2,1,0:T(8,128)(2,1)}), bf16[8,48,512]{2,1,0:T(8,128)(2,1)S(1)}, u32[]{:S(2)}, u32[]{:S(2)}) %all-to-all-start.1) | async-done | bytes 393248 | tf_op jit(solution)/shard_map/all_to_all | solution.py:147
  222.2 1.2 gather_fusion.1
  223.7 1.4 multiply_reduce_fusion
  (86 shorter events, 7.1 us)
Async XLA Ops:
  7.2 134.9 %copy-start = (bf16[256,2048]{1,0:T(8,128)(2,1)S(1)}, bf16[256,2048]{1,0:T(8,128)(2,1)}, u32[]{:S(2)}) copy-start(bf16[256,2048]{1,0:T(8,128)(2,1)} %param.21) | copy-start | bytes 3145732
  7.2 10.1 %copy-start.2 = (bf16[128,2048]{1,0:T(8,128)(2,1)S(1)}, bf16[128,2048]{1,0:T(8,128)(2,1)}, u32[]{:S(2)}) copy-start(bf16[128,2048]{1,0:T(8,128)(2,1)} %param.23) | copy-start | bytes 1572868
  7.2 10.3 %copy-start.5 = (f32[2048]{0:T(1024)S(1)}, f32[2048]{0:T(1024)}, u32[]{:S(2)}) copy-start(f32[2048]{0:T(1024)} %param.26) | copy-start | bytes 24580
  9.8 16.3 %collective-permute-start = (bf16[512,128]{0,1:T(8,128)(2,1)S(1)}, bf16[512,128]{0,1:T(8,128)(2,1)S(1)}, u32[]{:S(2)}, u32[]{:S(2)}) collective-permute-start(bf16[512,128]{0,1:T(8,128)(2,1)S(1)} %pad_maximum_fusion), channel_id=1, source_target_pairs={{0,4},{4,0},{8,12},{12,8},{16,20},{20,16},{24,28},{28,24},{1,5},{5... | collective-permute-start | bytes 393224 | tf_op jit(solution)/shard_map/ppermute | solution.py:101
  20.9 5.1 %copy-start.3 = (bf16[512,256]{1,0:T(8,128)(2,1)S(1)}, bf16[512,256]{1,0:T(8,128)(2,1)}, u32[]{:S(2)}) copy-start(bf16[512,256]{1,0:T(8,128)(2,1)} %param.16) | copy-start | bytes 786436
  20.9 7.5 %copy-start.7 = (f32[64]{0:T(128)S(1)}, f32[64]{0:T(128)}, u32[]{:S(2)}) copy-start(f32[64]{0:T(128)} %param.19) | copy-start | bytes 772
  20.9 123.5 %all-to-all-start = ((bf16[8,48,2048]{2,1,0:T(8,128)(2,1)}), bf16[8,48,2048]{2,1,0:T(8,128)(2,1)}, u32[]{:S(2)}, u32[]{:S(2)}) async-start(bf16[8,48,2048]{2,1,0:T(8,128)(2,1)} %bitcast.13), calls=%async_computation.1 | async-start | bytes 3145728 | tf_op jit(solution)/shard_map/all_to_all | solution.py:137
  25.9 148.7 %reduce-scatter.3.cloned.1.call-start = ((), (), s32[]{:S(2)}) async-start(), calls=%async_computation.4 | async-start | bytes 2621440 | tf_op jit(solution)/shard_map/reduce_scatter | solution.py:117
  26.3 30.9 %collective-permute-start.1 = (bf16[1024,128]{0,1:T(8,128)(2,1)S(1)}, bf16[1024,128]{0,1:T(8,128)(2,1)S(1)}, u32[]{:S(2)}, u32[]{:S(2)}) collective-permute-start(bf16[1024,128]{0,1:T(8,128)(2,1)S(1)} %maximum_select_fusion.2), channel_id=1, source_target_pairs={{0,8},{4,12},{8,0},{12,4},{16,24},{20,28},{24,16},{28,20},{1,9},{5... | collective-permute-start | bytes 786440 | tf_op jit(solution)/shard_map/ppermute | solution.py:101
  57.2 5.0 %copy-start.1 = (bf16[2048,128]{0,1:T(8,128)(2,1)}, bf16[2048,128]{0,1:T(8,128)(2,1)S(1)}, u32[]{:S(2)}) copy-start(bf16[2048,128]{0,1:T(8,128)(2,1)S(1)} %maximum_select_fusion.1) | copy-start | bytes 1572868
  57.3 27.9 %collective-permute-start.2 = (bf16[2048,128]{0,1:T(8,128)(2,1)S(1)}, bf16[2048,128]{0,1:T(8,128)(2,1)}, u32[]{:S(2)}, u32[]{:S(2)}) collective-permute-start(bf16[2048,128]{0,1:T(8,128)(2,1)S(1)} %maximum_select_fusion.1), channel_id=1, source_target_pairs={{0,16},{4,20},{8,24},{12,28},{16,0},{20,4},{24,8},{28,12},{1,17},{... | collective-permute-start | bytes 1572872 | tf_op jit(solution)/shard_map/ppermute | solution.py:101
  144.2 60.9 %reduce-scatter.5.cloned.1.call-start = ((), (), s32[]{:S(2)}) async-start(), calls=%async_computation.5 | async-start | bytes 1966080 | tf_op jit(solution)/shard_map/reduce_scatter | solution.py:144
  144.4 4.6 %copy-start.8 = (bf16[1,2048,1024]{2,1,0:T(8,128)(2,1)S(1)}, bf16[1,2048,1024]{2,1,0:T(8,128)(2,1)}, u32[]{:S(2)}) copy-start(bf16[1,2048,1024]{2,1,0:T(8,128)(2,1)} %param.28) | copy-start | bytes 12582916
  149.0 3.7 %copy-start.9 = (bf16[1,1024,2048]{2,1,0:T(8,128)(2,1)S(1)}, bf16[1,1024,2048]{2,1,0:T(8,128)(2,1)}, u32[]{:S(2)}) copy-start(bf16[1,1024,2048]{2,1,0:T(8,128)(2,1)} %param.29) | copy-start | bytes 12582916
  152.7 3.0 %copy-start.4 = (f32[128,2]{0,1:T(2,128)S(1)}, f32[128,2]{0,1:T(2,128)}, u32[]{:S(2)}) copy-start(f32[128,2]{0,1:T(2,128)} %param.25) | copy-start | bytes 3076
  155.7 54.9 %copy-start.6 = (f32[2048]{0:T(1024)S(1)}, f32[2048]{0:T(1024)}, u32[]{:S(2)}) copy-start(f32[2048]{0:T(1024)} %param.22) | copy-start | bytes 24580
  205.1 17.1 %all-to-all-start.1 = ((bf16[8,48,512]{2,1,0:T(8,128)(2,1)}), bf16[8,48,512]{2,1,0:T(8,128)(2,1)S(1)}, u32[]{:S(2)}, u32[]{:S(2)}) async-start(bf16[8,48,512]{2,1,0:T(8,128)(2,1)} %reduce-scatter.5.cloned.1.call-done), calls=%async_computation.3 | async-start | bytes 786432 | tf_op jit(solution)/shard_map/all_to_all | solution.py:147
Sparse Core Ops, SparseCore 0:
  144.3 30.2 reduce-scatter.2
  177.1 27.9 reduce-scatter.4
